TPU v7x, 32 devices: a whole 2x2x4 slice. The times are simulated.
32 devices in a mesh: ep: 8 (over z, core), tp: 4 (over y, x).
Axes of the slice: x: 2, y: 2, z: 4, core: 2. Of those that a mesh axis runs over, the one named last changes fastest.
Arguments:
- tokens: bfloat16 [256, 2048], P('ep', 'tp'), may hold values from -200 to 200
- routing: int32 [256, 4], P('ep'), may hold values from 0 to 15, all different within a row; in each aligned block of 32 rows (0 to 31, 32 to 63, ...) at most 8 rows name the same one
- gate_weights: float32 [256, 4], P('ep'), may hold values from 0.05 to 1
- norm_gain: float32 [2048], replicated, may hold values from 0.1 to 1.9
- w_gate: bfloat16 [16, 2048, 2048], P('ep', None, 'tp'), may hold values from -0.33007812 to 0.33007812
- w_up: bfloat16 [16, 2048, 2048], P('ep', None, 'tp'), may hold values from -0.33007812 to 0.33007812
- w_down: bfloat16 [16, 2048, 2048], P('ep', 'tp'), may hold values from -0.026489258 to 0.026489258
Outputs:
- mixed: bfloat16 [256, 2048], P('ep', 'tp')
Inputs may be any that keep to these rules, and one draw needn't show every extreme that they name: `routing`: each token names 4 different experts. Among the 32 tokens of one index of ep no expert is named more than 8 times, a bound that some block reaches.
All inputs are finite; a program needn't handle non-finite values.
Results may differ from a plain program's by a relative error of at most 0.015.
Values may be sent and summed in bfloat16 or wider, within the bound.
A program may use at most 128 MiB of HBM per device.

v0:
```python
import functools

import jax
import jax.numpy as jnp
from jax import lax
from jax.experimental import pallas as pl
from jax.experimental.pallas import tpu as pltpu
from jax.sharding import PartitionSpec as P

CAP = 8
MESH = pl.DeviceIdType.MESH

norm_eps = 1e-06
clamp_limit = 7.0
swish_alpha = 1.702


def partner(me, step, n):
    if n & (n - 1):
        return lax.rem(me + step, n)
    other, bit = 0, 1
    while bit < n:
        mine = (me // bit) % 2
        other = other + bit * ((1 - mine) if step & bit else mine)
        bit *= 2
    return other


def nearest(me, step, n):
    bound = n * n
    found = 0
    for at in range(n):
        by_distance = sorted(range(n), key=lambda other: (abs(other - at), other))
        apart = (me - at) * (me - at)
        found = found + by_distance[step] * (1 - lax.div(apart + (bound - 1), bound))
    return found


def kernel(
    n_ep,
    n_tp,
    tok_hbm,
    rout_hbm,
    gw_hbm,
    gain_hbm,
    wg_hbm,
    wu_hbm,
    wd_hbm,
    out_ref,
    tok_ref,
    rout_ref,
    gw_ref,
    gain_ref,
    wg,
    wu,
    wd,
    outgoing,
    rows,
    combine,
    acc_gate,
    acc_up,
    part,
    part_in,
    ret_out,
    ret_in,
    in_sem,
    w_sem,
    disp_send,
    disp_recv,
    gath_send,
    gath_recv,
    part_send,
    part_recv,
    ret_send,
    ret_recv,
):
    ep, tp = lax.axis_index("ep"), lax.axis_index("tp")
    n_exp, width, ff = wg_hbm.shape
    n_tok, cols = tok_ref.shape
    top = rout_ref.shape[0]
    chunk = n_exp * CAP
    slots = n_ep * chunk
    pair = 2 if n_ep % 2 == 0 else 1
    n_chip = n_ep // pair
    chip, core = lax.div(ep, pair), lax.rem(ep, pair)
    chips = [chip] + [nearest(chip, step, n_chip) for step in range(1, n_chip)]
    peers = []
    for step, other in enumerate(chips):
        for turn in range(pair):
            if step or turn:
                peers.append(other * pair + lax.rem(core + turn, pair))

    small = [
        pltpu.make_async_copy(src, dst, in_sem.at[i])
        for i, (src, dst) in enumerate(
            ((rout_hbm, rout_ref), (gw_hbm, gw_ref), (tok_hbm, tok_ref), (gain_hbm, gain_ref))
        )
    ]
    for copy in small:
        copy.start()

    barrier = pltpu.get_barrier_semaphore()
    for peer in peers:
        pl.semaphore_signal(barrier, inc=1, device_id=(peer, tp), device_id_type=MESH)
    for step in range(1, n_tp):
        pl.semaphore_signal(
            barrier, inc=1, device_id=(ep, partner(tp, step, n_tp)), device_id_type=MESH
        )

    loads = []
    for e in range(n_exp):
        for i, (src, dst) in enumerate(((wg_hbm, wg), (wu_hbm, wu), (wd_hbm, wd))):
            loads.append(pltpu.make_async_copy(src.at[e], dst.at[e], w_sem.at[i, e]))
    for load in loads:
        load.start()

    slot = lax.broadcasted_iota(jnp.int32, (slots, n_tok), 0)
    group, slot_rank = slot // CAP, slot % CAP
    slot_exp = (group % n_ep) * n_exp + group // n_ep
    named = jnp.zeros((slots, n_tok), jnp.float32)
    weight = jnp.zeros((slots, n_tok), jnp.float32)
    small[0].wait()
    small[1].wait()
    for k in range(top):
        hit = rout_ref[k : k + 1, :] == slot_exp
        named = named + jnp.where(hit, 1.0, 0.0)
        weight = weight + jnp.where(hit, gw_ref[k : k + 1, :], 0.0)
    earlier = jnp.where(
        lax.broadcasted_iota(jnp.int32, (n_tok, n_tok), 0)
        < lax.broadcasted_iota(jnp.int32, (n_tok, n_tok), 1),
        1.0,
        0.0,
    ).astype(jnp.bfloat16)
    rank = jnp.dot(named.astype(jnp.bfloat16), earlier, preferred_element_type=jnp.float32)
    placing = jnp.where(rank == slot_rank.astype(jnp.float32), named, 0.0)
    small[2].wait()
    sent = jnp.dot(
        placing.astype(jnp.bfloat16), tok_ref[...], preferred_element_type=jnp.float32
    )
    outgoing[...] = sent.astype(jnp.bfloat16).reshape(n_exp, n_ep, CAP, cols)
    for e in range(n_exp):
        rows[tp, e, ep] = outgoing[e, ep]

    pl.semaphore_wait(barrier, n_ep - 1 + n_tp - 1)

    def dispatch(peer, slot, e):
        return pltpu.make_async_remote_copy(
            src_ref=outgoing.at[e, peer],
            dst_ref=rows.at[tp, e, slot],
            send_sem=disp_send.at[e, peer],
            recv_sem=disp_recv.at[e, slot],
            device_id=(peer, tp),
            device_id_type=MESH,
        )

    def gather(src, peer, source_tp, e, s):
        return pltpu.make_async_remote_copy(
            src_ref=src,
            dst_ref=rows.at[source_tp, e, s],
            send_sem=gath_send.at[peer, e, s],
            recv_sem=gath_recv.at[source_tp, e, s],
            device_id=(ep, peer),
            device_id_type=MESH,
        )

    def reduce(peer, slot, e, c):
        return pltpu.make_async_remote_copy(
            src_ref=part.at[peer, e, c],
            dst_ref=part_in.at[slot, e, c],
            send_sem=part_send.at[peer, e, c],
            recv_sem=part_recv.at[slot, e, c],
            device_id=(ep, peer),
            device_id_type=MESH,
        )

    def give_back(peer, slot, e):
        return pltpu.make_async_remote_copy(
            src_ref=ret_out.at[e, peer],
            dst_ref=ret_in.at[e, slot],
            send_sem=ret_send.at[e, peer],
            recv_sem=ret_recv.at[e, slot],
            device_id=(peer, tp),
            device_id_type=MESH,
        )

    def finish(pre_gate, pre_up, factor, e):
        clamped = jnp.minimum(pre_gate * factor, clamp_limit)
        upper = jnp.clip(pre_up * factor, -clamp_limit, clamp_limit)
        hidden = (clamped * jax.nn.sigmoid(swish_alpha * clamped) * (upper + 1.0)).astype(
            jnp.bfloat16
        )
        loads[3 * e + 2].wait()
        for hop in reversed(range(n_tp)):
            q = partner(tp, hop, n_tp) if hop else tp
            at = pl.multiple_of(q * cols, cols)
            part[q, e] = (
                jnp.dot(hidden, wd[e, :, pl.ds(at, cols)], preferred_element_type=jnp.float32)
                .reshape(n_chip, pair * CAP, cols)
                .astype(jnp.bfloat16)
            )
            if hop:
                for c in chips[::-1]:
                    reduce(q, tp, e, c).start()

    for e in range(n_exp):
        for step in reversed(range(1, n_tp)):
            gather(outgoing.at[e, ep], partner(tp, step, n_tp), tp, e, ep).start()
        for peer in peers:
            dispatch(peer, ep, e).start()

    def take(j, e):
        wide = rows[j, e].astype(jnp.float32)
        at = pl.multiple_of(j * cols, cols)
        x = wide * gain_ref[:, pl.ds(at, cols)].reshape(1, 1, cols)
        x = x.reshape(n_ep * CAP, cols).astype(jnp.bfloat16)
        y = [
            jnp.dot(x, w[e, pl.ds(at, cols), :], preferred_element_type=jnp.float32)
            for w in (wg, wu)
        ]
        return y, jnp.sum(wide * wide, axis=2, keepdims=True)

    squares = []
    for e in range(n_exp):
        for s in peers:
            dispatch(s, s, e).wait_recv()
            for hop in reversed(range(1, n_tp)):
                gather(rows.at[tp, e, s], partner(tp, hop, n_tp), tp, e, s).start()
        if e == 0:
            small[3].wait()
        loads[3 * e].wait()
        loads[3 * e + 1].wait()
        (acc_gate[e], acc_up[e]), ssq = take(tp, e)
        squares.append(ssq)
    combine[...] = (placing * weight).T

    for e in range(n_exp):
        ssq = squares[e]
        gate, up = acc_gate[e], acc_up[e]
        for hop in range(1, n_tp):
            j = partner(tp, hop, n_tp)
            for s in [ep] + peers:
                gather(rows.at[tp, e, s], j, j, e, s).wait_recv()
            (more_gate, more_up), more = take(j, e)
            gate, up, ssq = gate + more_gate, up + more_up, ssq + more
        factor = lax.rsqrt(ssq / width + norm_eps).reshape(n_ep * CAP, 1)
        finish(gate, up, factor, e)

    for e in range(n_exp):
        for step in reversed(range(n_chip)):
            c = chips[step]
            total = part[tp, e, c].astype(jnp.float32)
            for hop in range(1, n_tp):
                j = partner(tp, hop, n_tp)
                reduce(j, j, e, c).wait_recv()
                total = total + part_in[j, e, c].astype(jnp.float32)
            both = total.reshape(pair, CAP, cols).astype(jnp.bfloat16)
            ret_out[e, pl.ds(c * pair, pair)] = both
            if step:
                for peer in peers[step * pair - 1 : (step + 1) * pair - 1]:
                    give_back(peer, ep, e).start()
            else:
                for peer in peers[: pair - 1]:
                    give_back(peer, ep, e).start()
                ret_in[e, ep] = ret_out[e, ep]

    both = combine[...]
    high = both.astype(jnp.bfloat16)
    low = (both - high.astype(jnp.float32)).astype(jnp.bfloat16)

    for e in range(n_exp):
        for peer in peers:
            dispatch(peer, ep, e).wait_send()
    for hop in range(1, n_tp):
        q = partner(tp, hop, n_tp)
        for e in range(n_exp):
            for s in range(n_ep):
                gather(rows.at[tp, e, s], q, tp, e, s).wait_send()
            for c in chips:
                reduce(q, tp, e, c).wait_send()
    for e in range(n_exp):
        for s in peers:
            give_back(s, s, e).wait_recv()
    back = ret_in[...].astype(jnp.float32).reshape(slots, cols).astype(jnp.bfloat16)
    out_ref[...] = (
        jnp.dot(high, back, preferred_element_type=jnp.float32)
        + jnp.dot(low, back, preferred_element_type=jnp.float32)
    ).astype(jnp.bfloat16)
    for e in range(n_exp):
        for peer in peers:
            give_back(peer, ep, e).wait_send()


def per_device(tokens, routing, gate_weights, norm_gain, w_gate, w_up, w_down):
    n_ep, n_tp = lax.axis_size("ep"), lax.axis_size("tp")
    n_exp, width, ff = w_gate.shape
    n_tok, cols = tokens.shape
    chunk = n_exp * CAP
    slots = n_ep * chunk
    pair = 2 if n_ep % 2 == 0 else 1
    pieces = (n_ep // pair, pair * CAP, cols)
    vmem = pl.BlockSpec(memory_space=pltpu.VMEM)
    hbm = pl.BlockSpec(memory_space=pltpu.HBM)
    bf16, f32 = jnp.bfloat16, jnp.float32
    dma = pltpu.SemaphoreType.DMA
    return pl.pallas_call(
        functools.partial(kernel, n_ep, n_tp),
        out_shape=pltpu.VMEM((n_tok, cols), bf16),
        in_specs=[hbm] * 7,
        out_specs=vmem,
        scratch_shapes=[
            pltpu.VMEM(tokens.shape, bf16),
            pltpu.VMEM(routing.shape[::-1], jnp.int32),
            pltpu.VMEM(gate_weights.shape[::-1], f32),
            pltpu.VMEM((1, width), f32),
            pltpu.VMEM(w_gate.shape, bf16),
            pltpu.VMEM(w_up.shape, bf16),
            pltpu.VMEM(w_down.shape, bf16),
            pltpu.VMEM((n_exp, n_ep, CAP, cols), bf16),
            pltpu.VMEM((n_tp, n_exp, n_ep, CAP, cols), bf16),
            pltpu.VMEM((n_tok, slots), f32),
            pltpu.VMEM((n_exp, n_ep * CAP, ff), f32),
            pltpu.VMEM((n_exp, n_ep * CAP, ff), f32),
            pltpu.VMEM((n_tp, n_exp, *pieces), bf16),
            pltpu.VMEM((n_tp, n_exp, *pieces), bf16),
            pltpu.VMEM((n_exp, n_ep, CAP, cols), bf16),
            pltpu.VMEM((n_exp, n_ep, CAP, cols), bf16),
            dma((4,)),
            dma((3, n_exp)),
            dma((n_exp, n_ep)),
            dma((n_exp, n_ep)),
            dma((n_tp, n_exp, n_ep)),
            dma((n_tp, n_exp, n_ep)),
            dma((n_tp, n_exp, n_ep // pair)),
            dma((n_tp, n_exp, n_ep // pair)),
            dma((n_exp, n_ep)),
            dma((n_exp, n_ep)),
        ],
        compiler_params=pltpu.CompilerParams(collective_id=0, has_side_effects=True),
    )(tokens, routing.T, gate_weights.T, norm_gain.reshape(1, width), w_gate, w_up, w_down)


def solution(mesh):
    in_specs = (
        P("ep", "tp"),
        P("ep", None),
        P("ep", None),
        P(),
        P("ep", None, "tp"),
        P("ep", None, "tp"),
        P("ep", "tp", None),
    )
    return jax.shard_map(
        per_device, mesh=mesh, in_specs=in_specs, out_specs=P("ep", "tp"), check_vma=False
    )
```

profile of v0, /device:TPU:0, one launch (start us, length us, event | category | flops | bytes accessed | tf_op | source)
XLA Modules:
  0.0 27.3 jit_solution(13350022576979009702)
XLA Ops:
  0.0 26.7 %shard_map.73 = bf16[32,512]{1,0:T(8,128)(2,1)S(1)} custom-call(bf16[32,512]{1,0:T(8,128)(2,1)} %tok_hbm.1, s32[4,32]{1,0:T(4,128)} %bitcast.4, f32[4,32]{1,0:T(4,128)} %bitcast.5, f32[1,2048]{1,0:T(1,128)} %bitcast.3, bf16[2,2048,512]{2,1,0:T(8,128)(2,1)} %wg_hbm.1, bf16[2,2048,512]{2,1,0:T(8,128)(2,1)} %wu_hbm.1, bf16[2,512,2048]{2,1,0:T(8,128)(2,1)} %wd_hbm.1), custom_call_target="tpu_custom_call" | custom-call | tf_op jit(solution)/shard_map/pallas_call | solution.py:305
  26.7 0.6 %copy.9 = bf16[32,512]{1,0:T(8,128)(2,1)} copy(bf16[32,512]{1,0:T(8,128)(2,1)S(1)} %shard_map.73) | data formatting | bytes 65536
where the time goes:
time: 27.5 us; the launch traced here: 27.3 us
  Pallas kernels  26.7 us (97%)
  local copies, waits for them, and re-layouts  0.62 us (2%)
    pallas_call x1, Pallas kernels, per_device(): pl.pallas_call(functools.partial(kernel, n_ep, n_tp), out_shape=pltpu.VME...  26.7 us
    unnamed x1, local copies, waits for them, and re-layouts  0.62 us

commit v1 on v0

v1 whole, which is shorter than its diff:
```python
import functools

import jax
import jax.numpy as jnp
from jax import lax
from jax.experimental import pallas as pl
from jax.experimental.pallas import tpu as pltpu
from jax.sharding import PartitionSpec as P

CAP = 8
MESH = pl.DeviceIdType.MESH

norm_eps = 1e-06
clamp_limit = 7.0
swish_alpha = 1.702


def partner(me, step, n):
    if n & (n - 1):
        return lax.rem(me + step, n)
    other, bit = 0, 1
    while bit < n:
        mine = (me // bit) % 2
        other = other + bit * ((1 - mine) if step & bit else mine)
        bit *= 2
    return other


def nearest(me, step, n):
    bound = n * n
    found = 0
    for at in range(n):
        by_distance = sorted(range(n), key=lambda other: (abs(other - at), other))
        apart = (me - at) * (me - at)
        found = found + by_distance[step] * (1 - lax.div(apart + (bound - 1), bound))
    return found


def kernel(
    n_ep,
    n_tp,
    tok_hbm,
    rout_hbm,
    gw_hbm,
    gain_hbm,
    wg_hbm,
    wu_hbm,
    wd_hbm,
    out_ref,
    tok_ref,
    rout_ref,
    gw_ref,
    gain_ref,
    wg,
    wu,
    wd,
    outgoing,
    rows,
    combine,
    acc_gate,
    acc_up,
    part,
    part_in,
    ret_out,
    ret_in,
    in_sem,
    w_sem,
    disp_send,
    disp_recv,
    gath_send,
    gath_recv,
    part_send,
    part_recv,
    ret_send,
    ret_recv,
):
    ep, tp = lax.axis_index("ep"), lax.axis_index("tp")
    n_exp, width, ff = wg_hbm.shape
    n_tok, cols = tok_ref.shape
    top = rout_ref.shape[0]
    slots = n_ep * n_exp * CAP
    pair = 2 if n_ep % 2 == 0 else 1
    n_chip = n_ep // pair
    chip, core = lax.div(ep, pair), lax.rem(ep, pair)
    chips = [chip] + [nearest(chip, step, n_chip) for step in range(1, n_chip)]
    cores = [lax.rem(core + turn, pair) for turn in range(pair)]
    peers = [chips[0] * pair + k for k in cores[1:]]
    peers += [other * pair + k for other in chips[1:] for k in cores]
    hops = list(range(1, n_tp))

    small = [
        pltpu.make_async_copy(src, dst, in_sem.at[i])
        for i, (src, dst) in enumerate(
            ((rout_hbm, rout_ref), (gw_hbm, gw_ref), (tok_hbm, tok_ref), (gain_hbm, gain_ref))
        )
    ]
    for copy in small:
        copy.start()

    barrier = pltpu.get_barrier_semaphore()
    for peer in peers[::-1]:
        pl.semaphore_signal(barrier, inc=1, device_id=(peer, tp), device_id_type=MESH)
    for hop in hops[::-1]:
        pl.semaphore_signal(
            barrier, inc=1, device_id=(ep, partner(tp, hop, n_tp)), device_id_type=MESH
        )

    loads = []
    for e in range(n_exp):
        for i, (src, dst) in enumerate(((wg_hbm, wg), (wu_hbm, wu), (wd_hbm, wd))):
            loads.append(pltpu.make_async_copy(src.at[e], dst.at[e], w_sem.at[i, e]))
    for load in loads:
        load.start()

    slot = lax.broadcasted_iota(jnp.int32, (slots, n_tok), 0)
    slot_exp, slot_rank = slot // CAP, slot % CAP
    named = jnp.zeros((slots, n_tok), jnp.float32)
    weight = jnp.zeros((slots, n_tok), jnp.float32)
    small[0].wait()
    small[1].wait()
    for k in range(top):
        hit = rout_ref[k : k + 1, :] == slot_exp
        named = named + jnp.where(hit, 1.0, 0.0)
        weight = weight + jnp.where(hit, gw_ref[k : k + 1, :], 0.0)
    earlier = jnp.where(
        lax.broadcasted_iota(jnp.int32, (n_tok, n_tok), 0)
        < lax.broadcasted_iota(jnp.int32, (n_tok, n_tok), 1),
        1.0,
        0.0,
    ).astype(jnp.bfloat16)
    rank = jnp.dot(named.astype(jnp.bfloat16), earlier, preferred_element_type=jnp.float32)
    placing = jnp.where(rank == slot_rank.astype(jnp.float32), named, 0.0)
    small[2].wait()
    sent = jnp.dot(
        placing.astype(jnp.bfloat16), tok_ref[...], preferred_element_type=jnp.float32
    )
    outgoing[...] = sent.astype(jnp.bfloat16).reshape(n_ep, n_exp, CAP, cols)
    rows[tp, ep] = outgoing[ep]

    pl.semaphore_wait(barrier, n_ep - 1 + n_tp - 1)

    def dispatch(peer):
        return pltpu.make_async_remote_copy(
            src_ref=outgoing.at[peer],
            dst_ref=rows.at[tp, ep],
            send_sem=disp_send,
            recv_sem=disp_recv.at[chip],
            device_id=(peer, tp),
            device_id_type=MESH,
        )

    def gather(src, hop, s, count, c):
        return pltpu.make_async_remote_copy(
            src_ref=src,
            dst_ref=rows.at[tp, pl.ds(s, count)],
            send_sem=gath_send,
            recv_sem=gath_recv.at[tp, c],
            device_id=(ep, partner(tp, hop, n_tp)),
            device_id_type=MESH,
        )

    def reduce(hop, e, c):
        q = partner(tp, hop, n_tp)
        return pltpu.make_async_remote_copy(
            src_ref=part.at[q, pl.ds(c * pair, pair), e],
            dst_ref=part_in.at[e, c, hop - 1],
            send_sem=part_send,
            recv_sem=part_recv.at[e, c],
            device_id=(ep, q),
            device_id_type=MESH,
        )

    def give_back(peer, e):
        return pltpu.make_async_remote_copy(
            src_ref=ret_out.at[peer, e],
            dst_ref=ret_in.at[ep, e],
            send_sem=ret_send,
            recv_sem=ret_recv,
            device_id=(peer, tp),
            device_id_type=MESH,
        )

    def landed(ref, sem):
        pltpu.make_async_copy(ref, ref, sem).wait()

    def finish(pre_gate, pre_up, factor, e):
        clamped = jnp.minimum(pre_gate * factor, clamp_limit)
        upper = jnp.clip(pre_up * factor, -clamp_limit, clamp_limit)
        hidden = (clamped * jax.nn.sigmoid(swish_alpha * clamped) * (upper + 1.0)).astype(
            jnp.bfloat16
        )
        loads[3 * e + 2].wait()
        for hop in hops[::-1] + [0]:
            q = partner(tp, hop, n_tp) if hop else tp
            at = pl.multiple_of(q * cols, cols)
            part[q, :, e] = (
                jnp.dot(hidden, wd[e, :, pl.ds(at, cols)], preferred_element_type=jnp.float32)
                .reshape(n_ep, CAP, cols)
                .astype(jnp.bfloat16)
            )
            if hop:
                for c in chips[::-1]:
                    reduce(hop, e, c).start()

    for peer in peers[::-1]:
        dispatch(peer).start()
    for hop in hops[::-1]:
        gather(outgoing.at[pl.ds(ep, 1)], hop, ep, 1, chip).start()

    def take(j, e):
        wide = rows[j, :, e].astype(jnp.float32)
        at = pl.multiple_of(j * cols, cols)
        x = wide * gain_ref[:, pl.ds(at, cols)].reshape(1, 1, cols)
        x = x.reshape(n_ep * CAP, cols).astype(jnp.bfloat16)
        y = [
            jnp.dot(x, w[e, pl.ds(at, cols), :], preferred_element_type=jnp.float32)
            for w in (wg, wu)
        ]
        return y, jnp.sum(wide * wide, axis=2, keepdims=True)

    for c in chips:
        if c is chips[0]:
            for s in peers[: pair - 1]:
                landed(rows.at[tp, s], disp_recv.at[c])
                for hop in hops[::-1]:
                    gather(rows.at[tp, pl.ds(s, 1)], hop, s, 1, c).start()
        else:
            here = rows.at[tp, pl.ds(c * pair, pair)]
            landed(here, disp_recv.at[c])
            for hop in hops[::-1]:
                gather(here, hop, c * pair, pair, c).start()
    small[3].wait()
    squares = []
    for e in range(n_exp):
        loads[3 * e].wait()
        loads[3 * e + 1].wait()
        (acc_gate[e], acc_up[e]), ssq = take(tp, e)
        squares.append(ssq)
    combine[...] = (placing * weight).T

    for e in range(n_exp):
        ssq = squares[e]
        gate, up = acc_gate[e], acc_up[e]
        for hop in hops:
            j = partner(tp, hop, n_tp)
            if e == 0:
                for c in chips:
                    landed(rows.at[j, pl.ds(c * pair, pair)], gath_recv.at[j, c])
            (more_gate, more_up), more = take(j, e)
            gate, up, ssq = gate + more_gate, up + more_up, ssq + more
        factor = lax.rsqrt(ssq / width + norm_eps).reshape(n_ep * CAP, 1)
        finish(gate, up, factor, e)

    for e in range(n_exp):
        for step in reversed(range(n_chip)):
            c = chips[step]
            landed(part_in.at[e, c], part_recv.at[e, c])
            total = part[tp, pl.ds(c * pair, pair), e].astype(jnp.float32)
            for hop in hops:
                total = total + part_in[e, c, hop - 1].astype(jnp.float32)
            ret_out[pl.ds(c * pair, pair), e] = total.astype(jnp.bfloat16)
            group = peers[step * pair - 1 : (step + 1) * pair - 1] if step else peers[: pair - 1]
            for peer in group:
                give_back(peer, e).start()
            if not step:
                ret_in[ep, e] = ret_out[ep, e]

    both = combine[...]
    high = both.astype(jnp.bfloat16)
    low = (both - high.astype(jnp.float32)).astype(jnp.bfloat16)

    others = pl.ds(0, n_ep - 1)
    landed(outgoing.at[others], disp_send)
    landed(rows.at[pl.ds(0, n_tp - 1)], gath_send)
    landed(part.at[pl.ds(0, n_tp - 1)], part_send)
    landed(ret_in.at[others], ret_recv)
    back = ret_in[...].reshape(slots, cols)
    out_ref[...] = (
        jnp.dot(high, back, preferred_element_type=jnp.float32)
        + jnp.dot(low, back, preferred_element_type=jnp.float32)
    ).astype(jnp.bfloat16)
    landed(ret_out.at[others], ret_send)


def per_device(tokens, routing, gate_weights, norm_gain, w_gate, w_up, w_down):
    n_ep, n_tp = lax.axis_size("ep"), lax.axis_size("tp")
    n_exp, width, ff = w_gate.shape
    n_tok, cols = tokens.shape
    slots = n_ep * n_exp * CAP
    pair = 2 if n_ep % 2 == 0 else 1
    n_chip = n_ep // pair
    vmem = pl.BlockSpec(memory_space=pltpu.VMEM)
    hbm = pl.BlockSpec(memory_space=pltpu.HBM)
    bf16, f32 = jnp.bfloat16, jnp.float32
    dma = pltpu.SemaphoreType.DMA
    return pl.pallas_call(
        functools.partial(kernel, n_ep, n_tp),
        out_shape=pltpu.VMEM((n_tok, cols), bf16),
        in_specs=[hbm] * 7,
        out_specs=vmem,
        scratch_shapes=[
            pltpu.VMEM(tokens.shape, bf16),
            pltpu.VMEM(routing.shape[::-1], jnp.int32),
            pltpu.VMEM(gate_weights.shape[::-1], f32),
            pltpu.VMEM((1, width), f32),
            pltpu.VMEM(w_gate.shape, bf16),
            pltpu.VMEM(w_up.shape, bf16),
            pltpu.VMEM(w_down.shape, bf16),
            pltpu.VMEM((n_ep, n_exp, CAP, cols), bf16),
            pltpu.VMEM((n_tp, n_ep, n_exp, CAP, cols), bf16),
            pltpu.VMEM((n_tok, slots), f32),
            pltpu.VMEM((n_exp, n_ep * CAP, ff), f32),
            pltpu.VMEM((n_exp, n_ep * CAP, ff), f32),
            pltpu.VMEM((n_tp, n_ep, n_exp, CAP, cols), bf16),
            pltpu.VMEM((n_exp, n_chip, n_tp - 1, pair, CAP, cols), bf16),
            pltpu.VMEM((n_ep, n_exp, CAP, cols), bf16),
            pltpu.VMEM((n_ep, n_exp, CAP, cols), bf16),
            dma((4,)),
            dma((3, n_exp)),
            dma,
            dma((n_chip,)),
            dma,
            dma((n_tp, n_chip)),
            dma,
            dma((n_exp, n_chip)),
            dma,
            dma,
        ],
        compiler_params=pltpu.CompilerParams(collective_id=0, has_side_effects=True),
    )(tokens, routing.T, gate_weights.T, norm_gain.reshape(1, width), w_gate, w_up, w_down)


def solution(mesh):
    in_specs = (
        P("ep", "tp"),
        P("ep", None),
        P("ep", None),
        P(),
        P("ep", None, "tp"),
        P("ep", None, "tp"),
        P("ep", "tp", None),
    )
    return jax.shard_map(
        per_device, mesh=mesh, in_specs=in_specs, out_specs=P("ep", "tp"), check_vma=False
    )
```

time: 27.5 us -> 27.8 us (1.011)
  Pallas kernels: 26.7 us -> 27 us
    pallas_call x1, Pallas kernels: 26.7 us -> 27 us  [per_device(): pl.pallas_call(functools.partial(kernel, n_ep, n_tp), out_shape=pltpu.VME...]
where the time goes in v1:
time: 27.8 us; the launch traced here: 27.6 us
  Pallas kernels  27 us (97%)
  local copies, waits for them, and re-layouts  0.62 us (2%)
    pallas_call x1, Pallas kernels, per_device(): pl.pallas_call(functools.partial(kernel, n_ep, n_tp), out_shape=pltpu.VME...  27 us
    unnamed x1, local copies, waits for them, and re-layouts  0.62 us

profile of v1, /device:TPU:0, one launch (start us, length us, event | category | flops | bytes accessed | tf_op | source)
XLA Modules:
  0.0 27.6 jit_solution(16965661750155598185)
XLA Ops:
  0.0 27.0 %shard_map.73 = bf16[32,512]{1,0:T(8,128)(2,1)S(1)} custom-call(bf16[32,512]{1,0:T(8,128)(2,1)} %tok_hbm.1, s32[4,32]{1,0:T(4,128)} %bitcast.4, f32[4,32]{1,0:T(4,128)} %bitcast.5, f32[1,2048]{1,0:T(1,128)} %bitcast.3, bf16[2,2048,512]{2,1,0:T(8,128)(2,1)} %wg_hbm.1, bf16[2,2048,512]{2,1,0:T(8,128)(2,1)} %wu_hbm.1, bf16[2,512,2048]{2,1,0:T(8,128)(2,1)} %wd_hbm.1), custom_call_target="tpu_custom_call" | custom-call | tf_op jit(solution)/shard_map/pallas_call | solution.py:296
  27.0 0.6 %copy.9 = bf16[32,512]{1,0:T(8,128)(2,1)} copy(bf16[32,512]{1,0:T(8,128)(2,1)S(1)} %shard_map.73) | data formatting | bytes 65536

commit v2 on v1

--- a/solution.py
+++ b/solution.py
@@ -113,48 +113,50 @@
         load.start()
 
     slot = lax.broadcasted_iota(jnp.int32, (slots, n_tok), 0)
-    slot_exp, slot_rank = slot // CAP, slot % CAP
+    group, slot_rank = slot // CAP, slot % CAP
+    slot_exp = (group % n_ep) * n_exp + group // n_ep
     named = jnp.zeros((slots, n_tok), jnp.float32)
     weight = jnp.zeros((slots, n_tok), jnp.float32)
+    earlier = jnp.where(
+        lax.broadcasted_iota(jnp.int32, (n_tok, n_tok), 0)
+        < lax.broadcasted_iota(jnp.int32, (n_tok, n_tok), 1),
+        1.0,
+        0.0,
+    ).astype(jnp.bfloat16)
     small[0].wait()
     small[1].wait()
     for k in range(top):
         hit = rout_ref[k : k + 1, :] == slot_exp
         named = named + jnp.where(hit, 1.0, 0.0)
         weight = weight + jnp.where(hit, gw_ref[k : k + 1, :], 0.0)
-    earlier = jnp.where(
-        lax.broadcasted_iota(jnp.int32, (n_tok, n_tok), 0)
-        < lax.broadcasted_iota(jnp.int32, (n_tok, n_tok), 1),
-        1.0,
-        0.0,
-    ).astype(jnp.bfloat16)
     rank = jnp.dot(named.astype(jnp.bfloat16), earlier, preferred_element_type=jnp.float32)
     placing = jnp.where(rank == slot_rank.astype(jnp.float32), named, 0.0)
     small[2].wait()
     sent = jnp.dot(
         placing.astype(jnp.bfloat16), tok_ref[...], preferred_element_type=jnp.float32
     )
-    outgoing[...] = sent.astype(jnp.bfloat16).reshape(n_ep, n_exp, CAP, cols)
-    rows[tp, ep] = outgoing[ep]
+    outgoing[...] = sent.astype(jnp.bfloat16).reshape(n_exp, n_ep, CAP, cols)
+    for e in range(n_exp):
+        rows[tp, e, ep] = outgoing[e, ep]
 
     pl.semaphore_wait(barrier, n_ep - 1 + n_tp - 1)
 
-    def dispatch(peer):
+    def dispatch(peer, e):
         return pltpu.make_async_remote_copy(
-            src_ref=outgoing.at[peer],
-            dst_ref=rows.at[tp, ep],
+            src_ref=outgoing.at[e, peer],
+            dst_ref=rows.at[tp, e, ep],
             send_sem=disp_send,
-            recv_sem=disp_recv.at[chip],
+            recv_sem=disp_recv.at[e, chip],
             device_id=(peer, tp),
             device_id_type=MESH,
         )
 
-    def gather(src, hop, s, count, c):
+    def gather(src, hop, e, s, count):
         return pltpu.make_async_remote_copy(
             src_ref=src,
-            dst_ref=rows.at[tp, pl.ds(s, count)],
+            dst_ref=rows.at[tp, e, pl.ds(s, count)],
             send_sem=gath_send,
-            recv_sem=gath_recv.at[tp, c],
+            recv_sem=gath_recv.at[e, tp],
             device_id=(ep, partner(tp, hop, n_tp)),
             device_id_type=MESH,
         )
@@ -162,7 +164,7 @@
     def reduce(hop, e, c):
         q = partner(tp, hop, n_tp)
         return pltpu.make_async_remote_copy(
-            src_ref=part.at[q, pl.ds(c * pair, pair), e],
+            src_ref=part.at[q, e, pl.ds(c * pair, pair)],
             dst_ref=part_in.at[e, c, hop - 1],
             send_sem=part_send,
             recv_sem=part_recv.at[e, c],
@@ -172,8 +174,8 @@
 
     def give_back(peer, e):
         return pltpu.make_async_remote_copy(
-            src_ref=ret_out.at[peer, e],
-            dst_ref=ret_in.at[ep, e],
+            src_ref=ret_out.at[e, peer],
+            dst_ref=ret_in.at[e, ep],
             send_sem=ret_send,
             recv_sem=ret_recv,
             device_id=(peer, tp),
@@ -182,6 +184,14 @@
 
     def landed(ref, sem):
         pltpu.make_async_copy(ref, ref, sem).wait()
+
+    def piece(hidden, q, e):
+        at = pl.multiple_of(q * cols, cols)
+        part[q, e] = (
+            jnp.dot(hidden, wd[e, :, pl.ds(at, cols)], preferred_element_type=jnp.float32)
+            .reshape(n_ep, CAP, cols)
+            .astype(jnp.bfloat16)
+        )
 
     def finish(pre_gate, pre_up, factor, e):
         clamped = jnp.minimum(pre_gate * factor, clamp_limit)
@@ -190,25 +200,28 @@
             jnp.bfloat16
         )
         loads[3 * e + 2].wait()
-        for hop in hops[::-1] + [0]:
-            q = partner(tp, hop, n_tp) if hop else tp
-            at = pl.multiple_of(q * cols, cols)
-            part[q, :, e] = (
-                jnp.dot(hidden, wd[e, :, pl.ds(at, cols)], preferred_element_type=jnp.float32)
-                .reshape(n_ep, CAP, cols)
-                .astype(jnp.bfloat16)
-            )
-            if hop:
-                for c in chips[::-1]:
-                    reduce(hop, e, c).start()
-
-    for peer in peers[::-1]:
-        dispatch(peer).start()
-    for hop in hops[::-1]:
-        gather(outgoing.at[pl.ds(ep, 1)], hop, ep, 1, chip).start()
+        if e < n_exp - 1:
+            down = jnp.dot(hidden, wd[e], preferred_element_type=jnp.float32).astype(jnp.bfloat16)
+            for q in range(n_tp):
+                part[q, e] = down[:, q * cols : (q + 1) * cols].reshape(n_ep, CAP, cols)
+        else:
+            for hop in hops[::-1]:
+                piece(hidden, partner(tp, hop, n_tp), e)
+        for c in chips[:0:-1]:
+            for hop in hops[::-1]:
+                reduce(hop, e, c).start()
+        if e == n_exp - 1:
+            piece(hidden, tp, e)
+
+    for e in range(n_exp):
+        for peer in peers:
+            dispatch(peer, e).start()
+    for e in range(n_exp):
+        for hop in hops[::-1]:
+            gather(outgoing.at[e, pl.ds(ep, 1)], hop, e, ep, 1).start()
 
     def take(j, e):
-        wide = rows[j, :, e].astype(jnp.float32)
+        wide = rows[j, e].astype(jnp.float32)
         at = pl.multiple_of(j * cols, cols)
         x = wide * gain_ref[:, pl.ds(at, cols)].reshape(1, 1, cols)
         x = x.reshape(n_ep * CAP, cols).astype(jnp.bfloat16)
@@ -218,20 +231,19 @@
         ]
         return y, jnp.sum(wide * wide, axis=2, keepdims=True)
 
-    for c in chips:
-        if c is chips[0]:
-            for s in peers[: pair - 1]:
-                landed(rows.at[tp, s], disp_recv.at[c])
-                for hop in hops[::-1]:
-                    gather(rows.at[tp, pl.ds(s, 1)], hop, s, 1, c).start()
-        else:
-            here = rows.at[tp, pl.ds(c * pair, pair)]
-            landed(here, disp_recv.at[c])
+    squares = []
+    for e in range(n_exp):
+        for s in peers[: pair - 1]:
+            landed(rows.at[tp, e, s], disp_recv.at[e, chip])
             for hop in hops[::-1]:
-                gather(here, hop, c * pair, pair, c).start()
-    small[3].wait()
-    squares = []
-    for e in range(n_exp):
+                gather(rows.at[tp, e, pl.ds(s, 1)], hop, e, s, 1).start()
+        for c in chips[1:]:
+            here = rows.at[tp, e, pl.ds(c * pair, pair)]
+            landed(here, disp_recv.at[e, c])
+            for hop in hops[::-1]:
+                gather(here, hop, e, c * pair, pair).start()
+        if not e:
+            small[3].wait()
         loads[3 * e].wait()
         loads[3 * e + 1].wait()
         (acc_gate[e], acc_up[e]), ssq = take(tp, e)
@@ -243,43 +255,45 @@
         gate, up = acc_gate[e], acc_up[e]
         for hop in hops:
             j = partner(tp, hop, n_tp)
-            if e == 0:
-                for c in chips:
-                    landed(rows.at[j, pl.ds(c * pair, pair)], gath_recv.at[j, c])
+            landed(rows.at[j, e], gath_recv.at[e, j])
             (more_gate, more_up), more = take(j, e)
             gate, up, ssq = gate + more_gate, up + more_up, ssq + more
         factor = lax.rsqrt(ssq / width + norm_eps).reshape(n_ep * CAP, 1)
         finish(gate, up, factor, e)
-
-    for e in range(n_exp):
-        for step in reversed(range(n_chip)):
-            c = chips[step]
-            landed(part_in.at[e, c], part_recv.at[e, c])
-            total = part[tp, pl.ds(c * pair, pair), e].astype(jnp.float32)
-            for hop in hops:
-                total = total + part_in[e, c, hop - 1].astype(jnp.float32)
-            ret_out[pl.ds(c * pair, pair), e] = total.astype(jnp.bfloat16)
-            group = peers[step * pair - 1 : (step + 1) * pair - 1] if step else peers[: pair - 1]
-            for peer in group:
-                give_back(peer, e).start()
-            if not step:
-                ret_in[ep, e] = ret_out[ep, e]
+    for e in range(n_exp):
+        for hop in hops[::-1]:
+            reduce(hop, e, chip).start()
+
+    turns = [(e, step) for e in range(n_exp) for step in range(n_chip - 1, 0, -1)]
+    turns += [(e, 0) for e in range(n_exp)]
+    for e, step in turns:
+        c = chips[step]
+        landed(part_in.at[e, c], part_recv.at[e, c])
+        total = part[tp, e, pl.ds(c * pair, pair)].astype(jnp.float32)
+        for hop in hops:
+            total = total + part_in[e, c, hop - 1].astype(jnp.float32)
+        ret_out[e, pl.ds(c * pair, pair)] = total.astype(jnp.bfloat16)
+        group = peers[step * pair - 1 : (step + 1) * pair - 1] if step else peers[: pair - 1]
+        for peer in group:
+            give_back(peer, e).start()
+        if not step:
+            ret_in[e, ep] = ret_out[e, ep]
 
     both = combine[...]
     high = both.astype(jnp.bfloat16)
     low = (both - high.astype(jnp.float32)).astype(jnp.bfloat16)
 
     others = pl.ds(0, n_ep - 1)
-    landed(outgoing.at[others], disp_send)
+    landed(outgoing.at[:, others], disp_send)
     landed(rows.at[pl.ds(0, n_tp - 1)], gath_send)
     landed(part.at[pl.ds(0, n_tp - 1)], part_send)
-    landed(ret_in.at[others], ret_recv)
+    landed(ret_in.at[:, others], ret_recv)
     back = ret_in[...].reshape(slots, cols)
     out_ref[...] = (
         jnp.dot(high, back, preferred_element_type=jnp.float32)
         + jnp.dot(low, back, preferred_element_type=jnp.float32)
     ).astype(jnp.bfloat16)
-    landed(ret_out.at[others], ret_send)
+    landed(ret_out.at[:, others], ret_send)
 
 
 def per_device(tokens, routing, gate_weights, norm_gain, w_gate, w_up, w_down):
@@ -306,21 +320,21 @@
             pltpu.VMEM(w_gate.shape, bf16),
             pltpu.VMEM(w_up.shape, bf16),
             pltpu.VMEM(w_down.shape, bf16),
-            pltpu.VMEM((n_ep, n_exp, CAP, cols), bf16),
-            pltpu.VMEM((n_tp, n_ep, n_exp, CAP, cols), bf16),
+            pltpu.VMEM((n_exp, n_ep, CAP, cols), bf16),
+            pltpu.VMEM((n_tp, n_exp, n_ep, CAP, cols), bf16),
             pltpu.VMEM((n_tok, slots), f32),
             pltpu.VMEM((n_exp, n_ep * CAP, ff), f32),
             pltpu.VMEM((n_exp, n_ep * CAP, ff), f32),
-            pltpu.VMEM((n_tp, n_ep, n_exp, CAP, cols), bf16),
+            pltpu.VMEM((n_tp, n_exp, n_ep, CAP, cols), bf16),
             pltpu.VMEM((n_exp, n_chip, n_tp - 1, pair, CAP, cols), bf16),
-            pltpu.VMEM((n_ep, n_exp, CAP, cols), bf16),
-            pltpu.VMEM((n_ep, n_exp, CAP, cols), bf16),
+            pltpu.VMEM((n_exp, n_ep, CAP, cols), bf16),
+            pltpu.VMEM((n_exp, n_ep, CAP, cols), bf16),
             dma((4,)),
             dma((3, n_exp)),
             dma,
-            dma((n_chip,)),
-            dma,
-            dma((n_tp, n_chip)),
+            dma((n_exp, n_chip)),
+            dma,
+            dma((n_exp, n_tp)),
             dma,
             dma((n_exp, n_chip)),
             dma,

time: 27.8 us -> 25.1 us (0.903)
  Pallas kernels: 27 us -> 24.3 us
    pallas_call x1, Pallas kernels: 27 us -> 24.3 us  [per_device(): pl.pallas_call(functools.partial(kernel, n_ep, n_tp), out_shape=pltpu.VME...]
where the time goes in v2:
time: 25.1 us; the launch traced here: 24.9 us
  Pallas kernels  24.3 us (97%)
  local copies, waits for them, and re-layouts  0.62 us (2%)
    pallas_call x1, Pallas kernels, per_device(): pl.pallas_call(functools.partial(kernel, n_ep, n_tp), out_shape=pltpu.VME...  24.3 us
    unnamed x1, local copies, waits for them, and re-layouts  0.62 us

profile of v2, /device:TPU:0, one launch (start us, length us, event | category | flops | bytes accessed | tf_op | source)
XLA Modules:
  0.0 24.9 jit_solution(11851897623890159741)
XLA Ops:
  0.0 24.3 %shard_map.73 = bf16[32,512]{1,0:T(8,128)(2,1)S(1)} custom-call(bf16[32,512]{1,0:T(8,128)(2,1)} %tok_hbm.1, s32[4,32]{1,0:T(4,128)} %bitcast.4, f32[4,32]{1,0:T(4,128)} %bitcast.5, f32[1,2048]{1,0:T(1,128)} %bitcast.3, bf16[2,2048,512]{2,1,0:T(8,128)(2,1)} %wg_hbm.1, bf16[2,2048,512]{2,1,0:T(8,128)(2,1)} %wu_hbm.1, bf16[2,512,2048]{2,1,0:T(8,128)(2,1)} %wd_hbm.1), custom_call_target="tpu_custom_call" | custom-call | tf_op jit(solution)/shard_map/pallas_call | solution.py:310
  24.3 0.6 %copy.9 = bf16[32,512]{1,0:T(8,128)(2,1)} copy(bf16[32,512]{1,0:T(8,128)(2,1)S(1)} %shard_map.73) | data formatting | bytes 65536

commit v3 on v2

--- a/solution.py
+++ b/solution.py
@@ -73,6 +73,7 @@
     part_recv,
     ret_send,
     ret_recv,
+    turn,
 ):
     ep, tp = lax.axis_index("ep"), lax.axis_index("tp")
     n_exp, width, ff = wg_hbm.shape
@@ -200,22 +201,23 @@
             jnp.bfloat16
         )
         loads[3 * e + 2].wait()
-        if e < n_exp - 1:
-            down = jnp.dot(hidden, wd[e], preferred_element_type=jnp.float32).astype(jnp.bfloat16)
-            for q in range(n_tp):
-                part[q, e] = down[:, q * cols : (q + 1) * cols].reshape(n_ep, CAP, cols)
-        else:
-            for hop in hops[::-1]:
-                piece(hidden, partner(tp, hop, n_tp), e)
-        for c in chips[:0:-1]:
-            for hop in hops[::-1]:
-                reduce(hop, e, c).start()
+        for hop in hops[::-1]:
+            piece(hidden, partner(tp, hop, n_tp), e)
+            if e < n_exp - 1:
+                for c in chips[:0:-1]:
+                    reduce(hop, e, c).start()
         if e == n_exp - 1:
-            piece(hidden, tp, e)
-
-    for e in range(n_exp):
-        for peer in peers:
-            dispatch(peer, e).start()
+            for c in chips[:0:-1]:
+                for hop in hops[::-1]:
+                    reduce(hop, e, c).start()
+        piece(hidden, tp, e)
+
+    for e in range(n_exp):
+        for k in cores[1:]:
+            dispatch(chip * pair + k, e).start()
+        for other in chips[1:]:
+            for k in range(pair):
+                dispatch(other * pair + k, e).start()
     for e in range(n_exp):
         for hop in hops[::-1]:
             gather(outgoing.at[e, pl.ds(ep, 1)], hop, e, ep, 1).start()
@@ -231,19 +233,40 @@
         ]
         return y, jnp.sum(wide * wide, axis=2, keepdims=True)
 
+    def forward(turns):
+        for e, step in turns:
+            c = chips[step]
+            if step == 0:
+                for s in peers[: pair - 1]:
+                    landed(rows.at[tp, e, s], disp_recv.at[e, c])
+                    for hop in hops[::-1]:
+                        gather(rows.at[tp, e, pl.ds(s, 1)], hop, e, s, 1).start()
+            else:
+                here = rows.at[tp, e, pl.ds(c * pair, pair)]
+                landed(here, disp_recv.at[e, c])
+                for hop in hops[::-1]:
+                    gather(here, hop, e, c * pair, pair).start()
+
+    soon = [(e, 0) for e in range(n_exp)] + [(0, step) for step in range(1, n_chip)]
+    later = [(e, step) for e in range(1, n_exp) for step in range(1, n_chip)]
+    forward(soon)
+    if pair == 2:
+
+        @pl.when(core == 0)
+        def _():
+            forward(later)
+            pl.semaphore_signal(turn, inc=1, device_id=(ep + 1, tp), device_id_type=MESH)
+
+        @pl.when(core != 0)
+        def _():
+            pl.semaphore_wait(turn, 1)
+            forward(later)
+
+    else:
+        forward(later)
     squares = []
-    for e in range(n_exp):
-        for s in peers[: pair - 1]:
-            landed(rows.at[tp, e, s], disp_recv.at[e, chip])
-            for hop in hops[::-1]:
-                gather(rows.at[tp, e, pl.ds(s, 1)], hop, e, s, 1).start()
-        for c in chips[1:]:
-            here = rows.at[tp, e, pl.ds(c * pair, pair)]
-            landed(here, disp_recv.at[e, c])
-            for hop in hops[::-1]:
-                gather(here, hop, e, c * pair, pair).start()
-        if not e:
-            small[3].wait()
+    small[3].wait()
+    for e in range(n_exp):
         loads[3 * e].wait()
         loads[3 * e + 1].wait()
         (acc_gate[e], acc_up[e]), ssq = take(tp, e)
@@ -339,6 +362,7 @@
             dma((n_exp, n_chip)),
             dma,
             dma,
+            pltpu.SemaphoreType.REGULAR,
         ],
         compiler_params=pltpu.CompilerParams(collective_id=0, has_side_effects=True),
     )(tokens, routing.T, gate_weights.T, norm_gain.reshape(1, width), w_gate, w_up, w_down)

time: 25.1 us -> 24.8 us (0.988)
  Pallas kernels: 24.3 us -> 24 us
    pallas_call x1, Pallas kernels: 24.3 us -> 24 us  [per_device(): pl.pallas_call(functools.partial(kernel, n_ep, n_tp), out_shape=pltpu.VME...]
where the time goes in v3:
time: 24.8 us; the launch traced here: 24.6 us
  Pallas kernels  24 us (97%)
  local copies, waits for them, and re-layouts  0.62 us (2%)
    pallas_call x1, Pallas kernels, per_device(): pl.pallas_call(functools.partial(kernel, n_ep, n_tp), out_shape=pltpu.VME...  24 us
    unnamed x1, local copies, waits for them, and re-layouts  0.62 us

profile of v3, /device:TPU:0, one launch (start us, length us, event | category | flops | bytes accessed | tf_op | source)
XLA Modules:
  0.0 24.6 jit_solution(16799589405851586165)
XLA Ops:
  0.0 24.0 %shard_map.73 = bf16[32,512]{1,0:T(8,128)(2,1)S(1)} custom-call(bf16[32,512]{1,0:T(8,128)(2,1)} %tok_hbm.1, s32[4,32]{1,0:T(4,128)} %bitcast.4, f32[4,32]{1,0:T(4,128)} %bitcast.5, f32[1,2048]{1,0:T(1,128)} %bitcast.3, bf16[2,2048,512]{2,1,0:T(8,128)(2,1)} %wg_hbm.1, bf16[2,2048,512]{2,1,0:T(8,128)(2,1)} %wu_hbm.1, bf16[2,512,2048]{2,1,0:T(8,128)(2,1)} %wd_hbm.1), custom_call_target="tpu_custom_call" | custom-call | tf_op jit(solution)/shard_map/pallas_call | solution.py:333
  24.0 0.6 %copy.9 = bf16[32,512]{1,0:T(8,128)(2,1)} copy(bf16[32,512]{1,0:T(8,128)(2,1)S(1)} %shard_map.73) | data formatting | bytes 65536

commit v4 on v3

--- a/solution.py
+++ b/solution.py
@@ -51,8 +51,7 @@
     rout_ref,
     gw_ref,
     gain_ref,
-    wg,
-    wu,
+    wgu,
     wd,
     outgoing,
     rows,
@@ -64,14 +63,14 @@
     ret_out,
     ret_in,
     in_sem,
-    w_sem,
-    disp_send,
+    gu_sem,
+    down_sem,
+    row_send,
     disp_recv,
     gath_send,
     gath_recv,
     part_send,
     part_recv,
-    ret_send,
     ret_recv,
     turn,
 ):
@@ -108,10 +107,12 @@
 
     loads = []
     for e in range(n_exp):
-        for i, (src, dst) in enumerate(((wg_hbm, wg), (wu_hbm, wu), (wd_hbm, wd))):
-            loads.append(pltpu.make_async_copy(src.at[e], dst.at[e], w_sem.at[i, e]))
+        loads.append(pltpu.make_async_copy(wg_hbm.at[e], wgu.at[0, e], gu_sem))
+        loads.append(pltpu.make_async_copy(wu_hbm.at[e], wgu.at[1, e], gu_sem))
     for load in loads:
         load.start()
+    down_load = pltpu.make_async_copy(wd_hbm, wd, down_sem)
+    down_load.start()
 
     slot = lax.broadcasted_iota(jnp.int32, (slots, n_tok), 0)
     group, slot_rank = slot // CAP, slot % CAP
@@ -146,7 +147,7 @@
         return pltpu.make_async_remote_copy(
             src_ref=outgoing.at[e, peer],
             dst_ref=rows.at[tp, e, ep],
-            send_sem=disp_send,
+            send_sem=row_send,
             recv_sem=disp_recv.at[e, chip],
             device_id=(peer, tp),
             device_id_type=MESH,
@@ -157,7 +158,7 @@
             src_ref=src,
             dst_ref=rows.at[tp, e, pl.ds(s, count)],
             send_sem=gath_send,
-            recv_sem=gath_recv.at[e, tp],
+            recv_sem=gath_recv.at[e, hop - 1],
             device_id=(ep, partner(tp, hop, n_tp)),
             device_id_type=MESH,
         )
@@ -177,7 +178,7 @@
         return pltpu.make_async_remote_copy(
             src_ref=ret_out.at[e, peer],
             dst_ref=ret_in.at[e, ep],
-            send_sem=ret_send,
+            send_sem=row_send,
             recv_sem=ret_recv,
             device_id=(peer, tp),
             device_id_type=MESH,
@@ -200,7 +201,8 @@
         hidden = (clamped * jax.nn.sigmoid(swish_alpha * clamped) * (upper + 1.0)).astype(
             jnp.bfloat16
         )
-        loads[3 * e + 2].wait()
+        if not e:
+            down_load.wait()
         for hop in hops[::-1]:
             piece(hidden, partner(tp, hop, n_tp), e)
             if e < n_exp - 1:
@@ -228,12 +230,12 @@
         x = wide * gain_ref[:, pl.ds(at, cols)].reshape(1, 1, cols)
         x = x.reshape(n_ep * CAP, cols).astype(jnp.bfloat16)
         y = [
-            jnp.dot(x, w[e, pl.ds(at, cols), :], preferred_element_type=jnp.float32)
-            for w in (wg, wu)
+            jnp.dot(x, wgu[i, e, pl.ds(at, cols), :], preferred_element_type=jnp.float32)
+            for i in range(2)
         ]
         return y, jnp.sum(wide * wide, axis=2, keepdims=True)
 
-    def forward(turns):
+    def forward(turns, await_rows=True, send=True):
         for e, step in turns:
             c = chips[step]
             if step == 0:
@@ -243,34 +245,37 @@
                         gather(rows.at[tp, e, pl.ds(s, 1)], hop, e, s, 1).start()
             else:
                 here = rows.at[tp, e, pl.ds(c * pair, pair)]
-                landed(here, disp_recv.at[e, c])
-                for hop in hops[::-1]:
-                    gather(here, hop, e, c * pair, pair).start()
+                if await_rows:
+                    landed(here, disp_recv.at[e, c])
+                if send:
+                    for hop in hops[::-1]:
+                        gather(here, hop, e, c * pair, pair).start()
 
     soon = [(e, 0) for e in range(n_exp)] + [(0, step) for step in range(1, n_chip)]
     later = [(e, step) for e in range(1, n_exp) for step in range(1, n_chip)]
     forward(soon)
     if pair == 2:
-
-        @pl.when(core == 0)
-        def _():
-            forward(later)
-            pl.semaphore_signal(turn, inc=1, device_id=(ep + 1, tp), device_id_type=MESH)
-
-        @pl.when(core != 0)
-        def _():
-            pl.semaphore_wait(turn, 1)
-            forward(later)
-
+        pl.when(core == 0)(lambda: forward(later))
+        pl.when(core != 0)(lambda: forward(later, send=False))
     else:
         forward(later)
     squares = []
     small[3].wait()
-    for e in range(n_exp):
-        loads[3 * e].wait()
-        loads[3 * e + 1].wait()
+    landed(wgu, gu_sem)
+    for e in range(n_exp):
         (acc_gate[e], acc_up[e]), ssq = take(tp, e)
         squares.append(ssq)
+    if pair == 2:
+
+        @pl.when(core == 0)
+        def _():
+            pl.semaphore_signal(turn, inc=1, device_id=(ep + 1, tp), device_id_type=MESH)
+
+        @pl.when(core != 0)
+        def _():
+            pl.semaphore_wait(turn, 1)
+            forward(later, await_rows=False)
+
     combine[...] = (placing * weight).T
 
     for e in range(n_exp):
@@ -278,7 +283,7 @@
         gate, up = acc_gate[e], acc_up[e]
         for hop in hops:
             j = partner(tp, hop, n_tp)
-            landed(rows.at[j, e], gath_recv.at[e, j])
+            landed(rows.at[j, e], gath_recv.at[e, (hop if n_tp & (n_tp - 1) == 0 else n_tp - hop) - 1])
             (more_gate, more_up), more = take(j, e)
             gate, up, ssq = gate + more_gate, up + more_up, ssq + more
         factor = lax.rsqrt(ssq / width + norm_eps).reshape(n_ep * CAP, 1)
@@ -307,7 +312,6 @@
     low = (both - high.astype(jnp.float32)).astype(jnp.bfloat16)
 
     others = pl.ds(0, n_ep - 1)
-    landed(outgoing.at[:, others], disp_send)
     landed(rows.at[pl.ds(0, n_tp - 1)], gath_send)
     landed(part.at[pl.ds(0, n_tp - 1)], part_send)
     landed(ret_in.at[:, others], ret_recv)
@@ -316,7 +320,7 @@
         jnp.dot(high, back, preferred_element_type=jnp.float32)
         + jnp.dot(low, back, preferred_element_type=jnp.float32)
     ).astype(jnp.bfloat16)
-    landed(ret_out.at[:, others], ret_send)
+    landed(rows.at[pl.ds(0, 2), :, others], row_send)
 
 
 def per_device(tokens, routing, gate_weights, norm_gain, w_gate, w_up, w_down):
@@ -340,8 +344,7 @@
             pltpu.VMEM(routing.shape[::-1], jnp.int32),
             pltpu.VMEM(gate_weights.shape[::-1], f32),
             pltpu.VMEM((1, width), f32),
-            pltpu.VMEM(w_gate.shape, bf16),
-            pltpu.VMEM(w_up.shape, bf16),
+            pltpu.VMEM((2, *w_gate.shape), bf16),
             pltpu.VMEM(w_down.shape, bf16),
             pltpu.VMEM((n_exp, n_ep, CAP, cols), bf16),
             pltpu.VMEM((n_tp, n_exp, n_ep, CAP, cols), bf16),
@@ -353,14 +356,14 @@
             pltpu.VMEM((n_exp, n_ep, CAP, cols), bf16),
             pltpu.VMEM((n_exp, n_ep, CAP, cols), bf16),
             dma((4,)),
-            dma((3, n_exp)),
+            dma,
+            dma,
             dma,
             dma((n_exp, n_chip)),
             dma,
-            dma((n_exp, n_tp)),
+            dma((n_exp, n_tp - 1)),
             dma,
             dma((n_exp, n_chip)),
-            dma,
             dma,
             pltpu.SemaphoreType.REGULAR,
         ],

time: 24.8 us -> 24.6 us (level)
  no operation moved by 1% of the time
where the time goes in v4:
time: 24.6 us; the launch traced here: 24.5 us
  Pallas kernels  23.8 us (97%)
  local copies, waits for them, and re-layouts  0.62 us (3%)
    pallas_call x1, Pallas kernels, per_device(): pl.pallas_call(functools.partial(kernel, n_ep, n_tp), out_shape=pltpu.VME...  23.8 us
    unnamed x1, local copies, waits for them, and re-layouts  0.62 us

profile of v4, /device:TPU:0, one launch (start us, length us, event | category | flops | bytes accessed | tf_op | source)
XLA Modules:
  0.0 24.5 jit_solution(10654920303783089428)
XLA Ops:
  0.0 23.8 %shard_map.73 = bf16[32,512]{1,0:T(8,128)(2,1)S(1)} custom-call(bf16[32,512]{1,0:T(8,128)(2,1)} %tok_hbm.1, s32[4,32]{1,0:T(4,128)} %bitcast.4, f32[4,32]{1,0:T(4,128)} %bitcast.5, f32[1,2048]{1,0:T(1,128)} %bitcast.3, bf16[2,2048,512]{2,1,0:T(8,128)(2,1)} %wg_hbm.1, bf16[2,2048,512]{2,1,0:T(8,128)(2,1)} %wu_hbm.1, bf16[2,512,2048]{2,1,0:T(8,128)(2,1)} %wd_hbm.1), custom_call_target="tpu_custom_call" | custom-call | tf_op jit(solution)/shard_map/pallas_call | solution.py:337
  23.8 0.6 %copy.9 = bf16[32,512]{1,0:T(8,128)(2,1)} copy(bf16[32,512]{1,0:T(8,128)(2,1)S(1)} %shard_map.73) | data formatting | bytes 65536

commit v5 on v4

--- a/solution.py
+++ b/solution.py
@@ -241,14 +241,14 @@
             if step == 0:
                 for s in peers[: pair - 1]:
                     landed(rows.at[tp, e, s], disp_recv.at[e, c])
-                    for hop in hops[::-1]:
+                    for hop in hops[:1] + hops[:0:-1]:
                         gather(rows.at[tp, e, pl.ds(s, 1)], hop, e, s, 1).start()
             else:
                 here = rows.at[tp, e, pl.ds(c * pair, pair)]
                 if await_rows:
                     landed(here, disp_recv.at[e, c])
                 if send:
-                    for hop in hops[::-1]:
+                    for hop in hops[:1] + hops[:0:-1]:
                         gather(here, hop, e, c * pair, pair).start()
 
     soon = [(e, 0) for e in range(n_exp)] + [(0, step) for step in range(1, n_chip)]

time: 24.6 us -> 24.4 us (level)
  no operation moved by 1% of the time
where the time goes in v5:
time: 24.4 us; the launch traced here: 24.3 us
  Pallas kernels  23.7 us (97%)
  local copies, waits for them, and re-layouts  0.62 us (3%)
    pallas_call x1, Pallas kernels, per_device(): pl.pallas_call(functools.partial(kernel, n_ep, n_tp), out_shape=pltpu.VME...  23.7 us
    unnamed x1, local copies, waits for them, and re-layouts  0.62 us

profile of v5, /device:TPU:0, one launch (start us, length us, event | category | flops | bytes accessed | tf_op | source)
XLA Modules:
  0.0 24.3 jit_solution(18313829973979874823)
XLA Ops:
  0.0 23.7 %shard_map.73 = bf16[32,512]{1,0:T(8,128)(2,1)S(1)} custom-call(bf16[32,512]{1,0:T(8,128)(2,1)} %tok_hbm.1, s32[4,32]{1,0:T(4,128)} %bitcast.4, f32[4,32]{1,0:T(4,128)} %bitcast.5, f32[1,2048]{1,0:T(1,128)} %bitcast.3, bf16[2,2048,512]{2,1,0:T(8,128)(2,1)} %wg_hbm.1, bf16[2,2048,512]{2,1,0:T(8,128)(2,1)} %wu_hbm.1, bf16[2,512,2048]{2,1,0:T(8,128)(2,1)} %wd_hbm.1), custom_call_target="tpu_custom_call" | custom-call | tf_op jit(solution)/shard_map/pallas_call | solution.py:337
  23.7 0.6 %copy.9 = bf16[32,512]{1,0:T(8,128)(2,1)} copy(bf16[32,512]{1,0:T(8,128)(2,1)S(1)} %shard_map.73) | data formatting | bytes 65536
